TPU v7x, 32 devices: a whole 2x2x4 slice. The times are simulated.
32 devices in a mesh: ep: 16 (over z, x, core), tp: 2 (over y).
Axes of the slice: x: 2, y: 2, z: 4, core: 2. Of those that a mesh axis runs over, the one named last changes fastest.
Arguments:
- mix_input: bfloat16 [8192, 1024], P(('ep', 'tp')), may hold values from -6 to 6
- pool_weight: bfloat16 [8, 128, 128], replicated, may hold values from -0.5 to 0.5
- pool_scale: float32 [1024], replicated, may hold values from 0.1 to 1.9
- out_weight: bfloat16 [1024, 2048], replicated, may hold values from -0.1875 to 0.1875
- moe_input: bfloat16 [2048, 2048], P('ep'), may hold values from -6 to 6
- moe_gain: float32 [2048], replicated, may hold values from 0.1 to 1.9
- group_router: bfloat16 [2048, 4], replicated, may hold values from -0.125 to 0.125
- inner_router: bfloat16 [2048, 16], replicated, may hold values from -0.125 to 0.125
- group_pick: int32 [2048], P('ep'), may hold values from 0 to 3
- inner_pick: int32 [2048, 2], P('ep'), may hold values from 0 to 3, all different within a row
- gate_weight: bfloat16 [16, 2048, 1024], P('ep', None, 'tp'), may hold values from -0.125 to 0.125
- up_weight: bfloat16 [16, 2048, 1024], P('ep', None, 'tp'), may hold values from -0.125 to 0.125
- down_weight: bfloat16 [16, 1024, 2048], P('ep', 'tp'), may hold values from -0.1875 to 0.1875
Outputs:
- mix_out: bfloat16 [8192, 2048], P(('ep', 'tp'))
- moe_out: bfloat16 [2048, 2048], P('ep', 'tp')
All inputs are finite; a program needn't handle non-finite values.
Results may differ from a plain program's by a relative error of at most 0.011.
Values may be sent and summed in bfloat16 or wider, within the bound.
A program may use at most 64 MiB of HBM per device.

v0:
```python
import functools

import jax
import jax.numpy as jnp
from jax import lax
from jax.experimental import pallas as pl
from jax.experimental.pallas import tpu as pltpu
from jax.sharding import PartitionSpec as P

MESH = pl.DeviceIdType.MESH
CHUNK = 4
LEAD = 16

WINDOW_MAX = 16


NORM_FLOOR = 0.25


def passed_along(value, axis, steps):
    count = lax.axis_size(axis)
    first, last = (max(0, -steps), min(count, count - steps))
    return lax.ppermute(value, axis, [(source, source + steps) for source in range(first, last)])


def trailing_means(extended, row_count, lead_rows, first_position):
    group_width = extended.shape[1] // 4
    position = first_position + jnp.arange(row_count, dtype=jnp.int32)
    pieces = []
    for scale_index in range(4):
        window = 2 ** (scale_index + 1)
        channel_block = extended[:, scale_index * group_width : (scale_index + 1) * group_width]
        window_sum = channel_block[lead_rows : lead_rows + row_count]
        for back_step in range(1, window):
            window_sum = (
                window_sum
                + channel_block[lead_rows - back_step : lead_rows - back_step + row_count]
            )
        divisor = jnp.minimum(position + 1, window).astype(jnp.float32)
        pieces.append(window_sum / divisor[:, None])
    return jnp.concatenate(pieces, axis=1)


def route_terms(group_logits, inner_logits, group_pick, inner_pick, per_group):
    group_ids = jnp.arange(group_logits.shape[1], dtype=jnp.int32)
    chosen = jnp.sum(
        jnp.where(group_pick[:, None] == group_ids[None, :], group_logits, 0.0), axis=1
    )
    group_share = 1.0 / jnp.sum(jnp.exp(group_logits - chosen[:, None]), axis=1)
    target = group_pick[:, None] * per_group + inner_pick
    expert_ids = jnp.arange(inner_logits.shape[1], dtype=jnp.int32)
    picked = jnp.sum(
        jnp.where(target[:, :, None] == expert_ids[None, None, :], inner_logits[:, None, :], 0.0),
        axis=2,
    )
    first_share = jax.nn.sigmoid(picked[:, 0] - picked[:, 1])
    route_weight = group_share[:, None] * jnp.stack([first_share, 1.0 - first_share], axis=1)
    return (target, route_weight)


def slot_terms(target, expert_count, capacity):
    expert_ids = jnp.arange(expert_count, dtype=jnp.int32)
    expert_hits = (target[:, :, None] == expert_ids[None, None, :]).astype(jnp.int32)
    per_token = jnp.sum(expert_hits, axis=1)
    earlier = jnp.cumsum(per_token, axis=0) - per_token
    route_rank = jnp.sum(expert_hits * earlier[:, None, :], axis=2)
    is_kept = route_rank < capacity
    slot_index = target * capacity + jnp.minimum(route_rank, capacity - 1)
    return (slot_index, is_kept)


def slot_sources(slot_index, is_kept, slot_count):
    token_ids = jnp.broadcast_to(
        jnp.arange(slot_index.shape[0], dtype=jnp.int32)[:, None], slot_index.shape
    )
    placed = jnp.where(is_kept, slot_index, slot_count).reshape(-1)
    source = jnp.zeros((slot_count,), jnp.int32).at[placed].set(token_ids.reshape(-1), mode="drop")
    slot_used = jnp.zeros((slot_count,), jnp.bool_).at[placed].set(True, mode="drop")
    return (source, slot_used)


def per_device(
    mix_input,
    pool_weight,
    pool_scale,
    out_weight,
    moe_input,
    moe_gain,
    group_router,
    inner_router,
    group_pick,
    inner_pick,
    gate_weight,
    up_weight,
    down_weight,
):
    row_count = mix_input.shape[0]
    reach_back = WINDOW_MAX - 1
    before = passed_along(mix_input[row_count - reach_back :], ("ep", "tp"), 1)
    extended = jnp.concatenate([before, mix_input], axis=0).astype(jnp.float32)
    first_position = lax.axis_index(("ep", "tp")) * row_count
    trailing = (
        trailing_means(extended, row_count, reach_back, first_position) - extended[reach_back:]
    )
    pooled = trailing.astype(jnp.bfloat16)
    groups, group_dim = (pool_weight.shape[0], pool_weight.shape[1])
    grouped = jnp.einsum(
        "tgc,gcd->tgd",
        pooled.reshape(row_count, groups, group_dim),
        pool_weight,
        preferred_element_type=jnp.float32,
    )
    grouped = (grouped.reshape(row_count, groups * group_dim) * pool_scale[None, :]).astype(
        jnp.bfloat16
    )
    mix_out = jnp.dot(grouped, out_weight, preferred_element_type=jnp.float32).astype(jnp.bfloat16)
    tokens, feature_width = moe_input.shape
    token_values = moe_input.astype(jnp.float32)
    norm_scale = lax.rsqrt(
        jnp.maximum(jnp.mean(token_values * token_values, axis=1, keepdims=True), NORM_FLOOR)
    )
    normed = (token_values * norm_scale * moe_gain[None, :]).astype(jnp.bfloat16)
    group_logits = jnp.dot(normed, group_router, preferred_element_type=jnp.float32)
    inner_logits = jnp.dot(normed, inner_router, preferred_element_type=jnp.float32)
    group_count = group_router.shape[1]
    expert_count = inner_router.shape[1]
    target, route_weight = route_terms(
        group_logits, inner_logits, group_pick, inner_pick, expert_count // group_count
    )
    capacity = 2 * inner_pick.shape[1] * tokens // expert_count
    slot_index, is_kept = slot_terms(target, expert_count, capacity)
    source, slot_used = slot_sources(slot_index, is_kept, expert_count * capacity)
    gate_local = gate_weight[0]
    up_local = up_weight[0]
    outgoing = jnp.where(slot_used[:, None], normed[source], jnp.zeros((), jnp.bfloat16))
    arrived = lax.all_to_all(outgoing, "ep", split_axis=0, concat_axis=0, tiled=True)
    gate_sum = jnp.dot(arrived, gate_local, preferred_element_type=jnp.float32)
    up_sum = jnp.dot(arrived, up_local, preferred_element_type=jnp.float32)
    hidden = (jax.nn.silu(gate_sum) * up_sum).astype(jnp.bfloat16)
    down_local = down_weight[0]
    expert_result = lax.psum_scatter(
        lax.dot_general(
            down_local, hidden, (((0,), (1,)), ((), ())), preferred_element_type=jnp.float32
        ).astype(jnp.bfloat16),
        "tp",
        scatter_dimension=0,
        tiled=True,
    )
    returned = lax.all_to_all(expert_result, "ep", split_axis=1, concat_axis=1, tiled=True)
    route_scale = jnp.where(is_kept, route_weight, 0.0).astype(jnp.bfloat16)
    route_scale = lax.optimization_barrier(route_scale).astype(jnp.float32)
    picked = jnp.take(returned, slot_index, axis=1).astype(jnp.float32)
    combined = jnp.sum(picked * route_scale[None, :, :], axis=2)
    moe_out = combined.T.astype(jnp.bfloat16)
    return (mix_out, moe_out)


def flipped(index, mask, count):
    total = 0
    bit = 1
    while bit < count:
        own = (index // bit) % 2
        total = total + bit * ((1 - own) if mask & bit else own)
        bit *= 2
    return total


def fused_kernel(
    n,
    capacity,
    per_group,
    mix_ref,
    pool_w_ref,
    pool_s_ref,
    out_w_hbm,
    moe_ref,
    gain_ref,
    group_rt_ref,
    inner_rt_ref,
    gp_ref,
    ip_ref,
    gate_hbm,
    up_hbm,
    down_hbm,
    mix_out_ref,
    moe_out_ref,
    out_w,
    gate_w,
    up_w,
    down_w,
    halo,
    pooled_v,
    grouped_v,
    normed_v,
    outgoing,
    arrived,
    part_own,
    part_send,
    part_recv,
    result,
    returned,
    near_part,
    near_back,
    near_own,
    near_send,
    near_recv,
    combine_w,
    load_sem,
    halo_sem,
    send_sem,
    recv_sem,
    swap_send,
    swap_recv,
    part_ssem,
    part_rsem,
    ret_send,
    ret_recv,
    near_sem,
):
    ep, tp = lax.axis_index("ep"), lax.axis_index("tp")
    other = 1 - tp
    total_devices = 2 * n
    linear = ep * 2 + tp
    following = lax.rem(linear + 1, total_devices)
    preceding = lax.rem(linear + total_devices - 1, total_devices)
    tokens, width = moe_ref.shape
    half = width // 2
    rows = mix_ref.shape[0]
    slots = n * capacity
    near = n // 2
    far_rows = near * capacity
    near_chunks = [(0, near)]
    far_chunks = [(first, CHUNK) for first in range(near, n, CHUNK)]
    side = ep // near

    barrier = pltpu.get_barrier_semaphore()
    greeted = [(flipped(ep, j, n), tp) for j in range(1, n)]
    greeted += [(ep, other), (following // 2, following % 2), (preceding // 2, preceding % 2)]
    for device in greeted:
        pl.semaphore_signal(barrier, inc=1, device_id=device, device_id_type=MESH)

    loads = [
        pltpu.make_async_copy(gate_hbm.at[0], gate_w, load_sem.at[0]),
        pltpu.make_async_copy(up_hbm.at[0], up_w, load_sem.at[1]),
        pltpu.make_async_copy(out_w_hbm, out_w, load_sem.at[2]),
        pltpu.make_async_copy(down_hbm.at[0, :, pl.ds(0, half)], down_w.at[0], load_sem.at[3]),
        pltpu.make_async_copy(down_hbm.at[0, :, pl.ds(half, half)], down_w.at[1], load_sem.at[4]),
    ]
    for index in (2, 0, 1, 3, 4):
        loads[index].start()

    values = moe_ref[...].astype(jnp.float32)
    scale = lax.rsqrt(
        jnp.maximum(jnp.sum(values * values, axis=1, keepdims=True) * (1.0 / width), NORM_FLOOR)
    )
    normed = (values * scale * gain_ref[...]).astype(jnp.bfloat16)
    normed_v[...] = normed

    group_pick = gp_ref[...]
    expert_count = inner_rt_ref.shape[0]
    targets = [group_pick * per_group + ip_ref[k : k + 1, :] for k in range(2)]
    expert_ids = lax.broadcasted_iota(jnp.int32, (expert_count, tokens), 0)
    hits = [expert_ids == target for target in targets]
    both = (hits[0].astype(jnp.float32) + hits[1].astype(jnp.float32)).astype(jnp.bfloat16)
    earlier_mask = (
        lax.broadcasted_iota(jnp.int32, (tokens, tokens), 0)
        < lax.broadcasted_iota(jnp.int32, (tokens, tokens), 1)
    ).astype(jnp.float32).astype(jnp.bfloat16)
    earlier = jnp.dot(both, earlier_mask, preferred_element_type=jnp.float32)
    slot_of = []
    for k in range(2):
        rank = jnp.sum(jnp.where(hits[k], earlier, 0.0), axis=0, keepdims=True).astype(jnp.int32)
        slot_of.append(jnp.where(rank < capacity, targets[k] * capacity + rank, -1))
    slot_ids = lax.broadcasted_iota(jnp.int32, (slots, tokens), 0)
    chosen = [slot_ids == slot for slot in slot_of]
    pick = jnp.where(chosen[0] | chosen[1], 1.0, 0.0).astype(jnp.bfloat16)
    for part in range(2):
        outgoing[part] = jnp.dot(
            pick, normed_v[:, part * half : (part + 1) * half], preferred_element_type=jnp.float32
        ).astype(jnp.bfloat16)

    pl.semaphore_wait(barrier, len(greeted))

    own_rows = pl.ds(pl.multiple_of(ep * capacity, capacity), capacity)
    halo_copy = pltpu.make_async_remote_copy(
        src_ref=mix_ref.at[pl.ds(rows - LEAD, LEAD)],
        dst_ref=halo,
        send_sem=halo_sem.at[0],
        recv_sem=halo_sem.at[1],
        device_id=(following // 2, following % 2),
        device_id_type=MESH,
    )
    halo_copy.start()

    def rows_of(index):
        return pl.ds(pl.multiple_of(index * capacity, capacity), capacity)

    def dispatch(j):
        there = flipped(ep, j, n)
        if j < near:
            src, dst = outgoing.at[:, rows_of(there)], arrived.at[:, own_rows]
        else:
            src, dst = outgoing.at[tp, rows_of(there)], arrived.at[tp, own_rows]
        return pltpu.make_async_remote_copy(
            src_ref=src,
            dst_ref=dst,
            send_sem=send_sem.at[j],
            recv_sem=recv_sem.at[j],
            device_id=(there, tp),
            device_id_type=MESH,
        )

    def swap(j):
        there = flipped(ep, j, n)
        return pltpu.make_async_remote_copy(
            src_ref=arrived.at[tp, rows_of(there)],
            dst_ref=arrived.at[tp, rows_of(there)],
            send_sem=swap_send.at[j],
            recv_sem=swap_recv.at[j],
            device_id=(ep, other),
            device_id_type=MESH,
        )

    def chunk_span(c):
        first, size = c
        start = flipped(ep // size, first // size, n // size) * size * capacity
        return pl.ds(pl.multiple_of(start, size * capacity), size * capacity)

    def half_rows_of(index):
        return rows_of(index % near)

    def half_span(c):
        first, size = c
        start = (flipped(ep // size, first // size, n // size) % (near // size)) * size * capacity
        return pl.ds(pl.multiple_of(start, size * capacity), size * capacity)

    def partial_copy(j):
        block = half_rows_of(flipped(ep, j, n))
        return pltpu.make_async_remote_copy(
            src_ref=part_send.at[block],
            dst_ref=part_recv.at[block],
            send_sem=part_ssem.at[j],
            recv_sem=part_rsem.at[j],
            device_id=(ep, other),
            device_id_type=MESH,
        )

    def give_back(j):
        there = flipped(ep, j, n)
        if j < near:
            src, dst = near_part.at[:, half_rows_of(there)], near_back.at[:, half_rows_of(ep)]
        else:
            src, dst = result.at[half_rows_of(there)], returned.at[half_rows_of(ep)]
        return pltpu.make_async_remote_copy(
            src_ref=src,
            dst_ref=dst,
            send_sem=ret_send.at[j],
            recv_sem=ret_recv.at[j],
            device_id=(there, tp),
            device_id_type=MESH,
        )

    near_copy = pltpu.make_async_remote_copy(
        src_ref=near_send,
        dst_ref=near_recv,
        send_sem=near_sem.at[0],
        recv_sem=near_sem.at[1],
        device_id=(ep, other),
        device_id_type=MESH,
    )

    def members(c):
        return [j for j in range(c[0], c[0] + c[1]) if j]

    for j in range(1, n):
        dispatch(j).start()
    arrived[:, own_rows] = outgoing[:, own_rows]

    def contract(left, right):
        return lax.dot_general(
            left, right, (((1,), (1,)), ((), ())), preferred_element_type=jnp.float32
        )

    group_logits = contract(group_rt_ref[...], normed_v[...])
    inner_logits = contract(inner_rt_ref[...], normed_v[...])
    group_ids = lax.broadcasted_iota(jnp.int32, group_logits.shape, 0)
    own_logit = jnp.sum(
        jnp.where(group_ids == group_pick, group_logits, 0.0), axis=0, keepdims=True
    )
    share = 1.0 / jnp.sum(jnp.exp(group_logits - own_logit), axis=0, keepdims=True)
    picked = [
        jnp.sum(jnp.where(hit, inner_logits, 0.0), axis=0, keepdims=True) for hit in hits
    ]
    first = jax.nn.sigmoid(picked[0] - picked[1])
    weights = [
        (share * value).astype(jnp.bfloat16).astype(jnp.float32) for value in (first, 1.0 - first)
    ]
    spread = jnp.where(chosen[0], weights[0], 0.0) + jnp.where(chosen[1], weights[1], 0.0)
    for part in range(2):
        combine_w[part] = spread[part * far_rows : (part + 1) * far_rows].T.astype(jnp.bfloat16)

    def mixer():
        halo_copy.wait()
        group_width = mix_ref.shape[1] // 4
        position = linear * rows + lax.broadcasted_iota(jnp.int32, (rows, 1), 0)
        is_first = linear == 0
        for index in range(4):
            window = 2 ** (index + 1)
            lanes = slice(index * group_width, (index + 1) * group_width)
            lead = jnp.where(is_first, 0.0, halo[:, lanes].astype(jnp.float32))
            body = mix_ref[:, lanes].astype(jnp.float32)
            sums = jnp.concatenate([lead, body], axis=0)
            shift = 1
            while shift < window:
                sums = sums + pltpu.roll(sums, shift, 0)
                shift *= 2
            inverse = 1.0 / jnp.minimum(position + 1, window).astype(jnp.float32)
            pooled_v[:, lanes] = (sums[LEAD:] * inverse - body).astype(jnp.bfloat16)
        group_dim = pool_w_ref.shape[1]
        for g in range(pool_w_ref.shape[0]):
            lanes = slice(g * group_dim, (g + 1) * group_dim)
            product = jnp.dot(pooled_v[:, lanes], pool_w_ref[g], preferred_element_type=jnp.float32)
            grouped_v[:, lanes] = (product * pool_s_ref[:, lanes]).astype(jnp.bfloat16)
        loads[2].wait()
        tile = 512

        @pl.loop(0, mix_out_ref.shape[1] // tile)
        def _(step):
            lanes = pl.ds(pl.multiple_of(step * tile, tile), tile)
            mix_out_ref[:, lanes] = jnp.dot(
                grouped_v[...], out_w[:, lanes], preferred_element_type=jnp.float32
            ).astype(jnp.bfloat16)

    def expert(c):
        span = chunk_span(c)
        sums = []
        for weight in (gate_w, up_w):
            sums.append(
                jnp.dot(arrived[0, span], weight[:half], preferred_element_type=jnp.float32)
                + jnp.dot(arrived[1, span], weight[half:], preferred_element_type=jnp.float32)
            )
        hidden = (sums[0] / (1.0 + jnp.exp(-sums[0])) * sums[1]).astype(jnp.bfloat16)

        def part(index):
            return jnp.dot(
                hidden, down_w[index], preferred_element_type=jnp.float32
            ).astype(jnp.bfloat16)

        span = half_span(c)
        if c[0] < near:
            near_part[0, span] = part(0)
            near_part[1, span] = part(1)
            for j in members(c):
                give_back(j).start()
            if c[0] == 0:
                block = half_rows_of(ep)
                near_back[:, block] = near_part[:, block]
        else:
            part_send[span] = part(other)
            for j in members(c):
                partial_copy(j).start()
            part_own[span] = part(tp)

    def finish(c):
        for j in members(c):
            finish_one(j)

    def finish_one(j):
        block = half_rows_of(flipped(ep, j, n))
        partial_copy(j).wait_recv()
        result[block] = (
            part_own[block].astype(jnp.float32) + part_recv[block].astype(jnp.float32)
        ).astype(jnp.bfloat16)
        give_back(j).start()

    def arrive(c):
        for j in members(c):
            dispatch(j).wait_recv()
            if j >= near:
                swap(j).start()

    def swapped(c):
        for j in members(c):
            swap(j).wait_recv()

    mixer()
    for index in (0, 1, 3, 4):
        loads[index].wait()
    for c in near_chunks:
        arrive(c)
        expert(c)
    unfinished = []
    for c in far_chunks:
        for j in members(c):
            dispatch(j).wait_recv()
            swap(j).start()
            if unfinished:
                finish_one(unfinished.pop(0))
        swapped(c)
        expert(c)
        unfinished += members(c)
    for j in unfinished:
        finish_one(j)
    for j in range(1, near):
        give_back(j).wait_recv()
    near_send[...] = jnp.dot(
        combine_w[side], near_back[other], preferred_element_type=jnp.float32
    ).astype(jnp.bfloat16)
    near_copy.start()
    near_own[...] = jnp.dot(combine_w[side], near_back[tp], preferred_element_type=jnp.float32)
    near_copy.wait_recv()
    near_own[...] += near_recv[...].astype(jnp.float32)
    for j in range(near, n):
        give_back(j).wait_recv()
    moe_out_ref[...] = (
        near_own[...]
        + jnp.dot(combine_w[1 - side], returned[...], preferred_element_type=jnp.float32)
    ).astype(jnp.bfloat16)
    near_copy.wait_send()
    for j in range(1, n):
        dispatch(j).wait_send()
        give_back(j).wait_send()
        if j >= near:
            swap(j).wait_send()
            partial_copy(j).wait_send()


def fused(
    mix_input,
    pool_weight,
    pool_scale,
    out_weight,
    moe_input,
    moe_gain,
    group_router,
    inner_router,
    group_pick,
    inner_pick,
    gate_weight,
    up_weight,
    down_weight,
):
    n = lax.axis_size("ep")
    tokens, width = moe_input.shape
    rows, channels = mix_input.shape
    expert_count = inner_router.shape[1]
    capacity = 2 * inner_pick.shape[1] * tokens // expert_count
    half = width // 2
    slots = n * capacity
    hidden = gate_weight.shape[2]
    far_rows = slots // 2
    bf16 = jnp.bfloat16
    vmem = pl.BlockSpec(memory_space=pltpu.VMEM)
    hbm = pl.BlockSpec(memory_space=pl.ANY)
    dma = pltpu.SemaphoreType.DMA
    return pl.pallas_call(
        functools.partial(
            fused_kernel, n, capacity, expert_count // group_router.shape[1]
        ),
        out_shape=(
            pltpu.VMEM((rows, out_weight.shape[1]), bf16),
            pltpu.VMEM((tokens, half), bf16),
        ),
        in_specs=[vmem, vmem, vmem, hbm] + [vmem] * 6 + [hbm] * 3,
        out_specs=(vmem, vmem),
        scratch_shapes=[
            pltpu.VMEM(out_weight.shape, bf16),
            pltpu.VMEM((width, hidden), bf16),
            pltpu.VMEM((width, hidden), bf16),
            pltpu.VMEM((2, hidden, half), bf16),
            pltpu.VMEM((LEAD, channels), bf16),
            pltpu.VMEM((rows, channels), bf16),
            pltpu.VMEM((rows, channels), bf16),
            pltpu.VMEM((tokens, width), bf16),
            pltpu.VMEM((2, slots, half), bf16),
            pltpu.VMEM((2, slots, half), bf16),
            pltpu.VMEM((far_rows, half), bf16),
            pltpu.VMEM((far_rows, half), bf16),
            pltpu.VMEM((far_rows, half), bf16),
            pltpu.VMEM((far_rows, half), bf16),
            pltpu.VMEM((far_rows, half), bf16),
            pltpu.VMEM((2, far_rows, half), bf16),
            pltpu.VMEM((2, far_rows, half), bf16),
            pltpu.VMEM((tokens, half), jnp.float32),
            pltpu.VMEM((tokens, half), bf16),
            pltpu.VMEM((tokens, half), bf16),
            pltpu.VMEM((2, tokens, far_rows), bf16),
            dma((5,)),
            dma((2,)),
            dma((n,)),
            dma((n,)),
            dma((n,)),
            dma((n,)),
            dma((n,)),
            dma((n,)),
            dma((n,)),
            dma((n,)),
            dma((2,)),
        ],
        compiler_params=pltpu.CompilerParams(
            collective_id=0, has_side_effects=True, vmem_limit_bytes=60 * 1024 * 1024
        ),
    )(
        mix_input,
        pool_weight,
        pool_scale[None, :],
        out_weight,
        moe_input,
        moe_gain[None, :],
        group_router.T,
        inner_router.T,
        group_pick[None, :],
        inner_pick.T,
        gate_weight,
        up_weight,
        down_weight,
    )


def step(*arrays):
    mix_input, moe_input, inner_router, inner_pick = arrays[0], arrays[4], arrays[7], arrays[9]
    n, n_tp = lax.axis_size("ep"), lax.axis_size("tp")
    capacity = 2 * inner_pick.shape[1] * moe_input.shape[0] // inner_router.shape[1]
    fits = (
        n_tp == 2
        and inner_pick.shape[1] == 2
        and n & (n - 1) == 0
        and n >= 2 * CHUNK
        and inner_router.shape[1] == n
        and capacity % 16 == 0
        and mix_input.shape[0] >= LEAD
    )
    return fused(*arrays) if fits else per_device(*arrays)


def solution(mesh):
    in_specs = (
        P(("ep", "tp"), None),
        P(),
        P(),
        P(),
        P("ep", None),
        P(),
        P(),
        P(),
        P("ep"),
        P("ep", None),
        P("ep", None, "tp"),
        P("ep", None, "tp"),
        P("ep", "tp", None),
    )
    out_specs = (P(("ep", "tp"), None), P("ep", "tp"))
    return jax.shard_map(
        step, mesh=mesh, in_specs=in_specs, out_specs=out_specs, check_vma=False
    )
```

profile of v0, /device:TPU:0, one launch (start us, length us, event | category | flops | bytes accessed | tf_op | source)
XLA Modules:
  0.0 66.6 jit_solution(158657711040071450)
XLA Ops:
  0.6 64.2 %shard_map.140 = (bf16[256,2048]{1,0:T(8,128)(2,1)S(1)}, bf16[128,1024]{1,0:T(8,128)(2,1)S(1)}) custom-call(bf16[256,1024]{1,0:T(8,128)(2,1)} %mix_ref.1, bf16[8,128,128]{2,1,0:T(8,128)(2,1)} %pool_w_ref.1, f32[1,1024]{1,0:T(1,128)} %bitcast.9, bf16[1024,2048]{1,0:T(8,128)(2,1)} %out_w_hbm.1, bf16[128,2048]{1,0:T(8,128)(2,1)} %moe_ref.1, f32[1,2048]{1,0:T(1,128)} %bitcast.8, ...), custom_call_target="tpu_custom_call" | custom-call | tf_op jit(solution)/shard_map/pallas_call | solution.py:556
  64.9 1.0 %copy.17 = bf16[256,2048]{1,0:T(8,128)(2,1)} copy(bf16[256,2048]{1,0:T(8,128)(2,1)S(1)} %get-tuple-element.2) | data formatting | bytes 2097152
  65.9 0.7 %copy.18 = bf16[128,1024]{1,0:T(8,128)(2,1)} copy(bf16[128,1024]{1,0:T(8,128)(2,1)S(1)} %get-tuple-element.3) | data formatting | bytes 524288
where the time goes:
time: 66.7 us; the launch traced here: 66.6 us
  Pallas kernels  64.2 us (96%)
  local copies, waits for them, and re-layouts  1.67 us (3%)
    pallas_call x1, Pallas kernels, fused(): pl.pallas_call(functools.partial(fused_kernel, n, capacity, expert_count...  64.2 us
    unnamed x2, local copies, waits for them, and re-layouts  1.67 us

commit v1 on v0

--- a/solution.py
+++ b/solution.py
@@ -199,11 +199,6 @@
     part_recv,
     result,
     returned,
-    near_part,
-    near_back,
-    near_own,
-    near_send,
-    near_recv,
     combine_w,
     load_sem,
     halo_sem,
@@ -215,7 +210,6 @@
     part_rsem,
     ret_send,
     ret_recv,
-    near_sem,
 ):
     ep, tp = lax.axis_index("ep"), lax.axis_index("tp")
     other = 1 - tp
@@ -228,10 +222,8 @@
     rows = mix_ref.shape[0]
     slots = n * capacity
     near = n // 2
-    far_rows = near * capacity
-    near_chunks = [(0, near)]
-    far_chunks = [(first, CHUNK) for first in range(near, n, CHUNK)]
-    side = ep // near
+    low, high = (ep // CHUNK) % 2, (ep // near) % 2
+    inner = low + high - 2 * low * high
 
     barrier = pltpu.get_barrier_semaphore()
     greeted = [(flipped(ep, j, n), tp) for j in range(1, n)]
@@ -246,7 +238,7 @@
         pltpu.make_async_copy(down_hbm.at[0, :, pl.ds(0, half)], down_w.at[0], load_sem.at[3]),
         pltpu.make_async_copy(down_hbm.at[0, :, pl.ds(half, half)], down_w.at[1], load_sem.at[4]),
     ]
-    for index in (2, 0, 1, 3, 4):
+    for index in (0, 1, 3, 4, 2):
         loads[index].start()
 
     values = moe_ref[...].astype(jnp.float32)
@@ -295,9 +287,16 @@
     def rows_of(index):
         return pl.ds(pl.multiple_of(index * capacity, capacity), capacity)
 
-    def dispatch(j):
-        there = flipped(ep, j, n)
-        if j < near:
+    def partner(k):
+        there = flipped(ep, k, n)
+        if k < near:
+            return k, there
+        shift = CHUNK if k < near + CHUNK else -CHUNK
+        return k + inner * shift, there + inner * (CHUNK - 2 * CHUNK * ((there // CHUNK) % 2))
+
+    def dispatch(k):
+        j, there = partner(k)
+        if k < near:
             src, dst = outgoing.at[:, rows_of(there)], arrived.at[:, own_rows]
         else:
             src, dst = outgoing.at[tp, rows_of(there)], arrived.at[tp, own_rows]
@@ -310,8 +309,8 @@
             device_id_type=MESH,
         )
 
-    def swap(j):
-        there = flipped(ep, j, n)
+    def swap(k):
+        j, there = partner(k)
         return pltpu.make_async_remote_copy(
             src_ref=arrived.at[tp, rows_of(there)],
             dst_ref=arrived.at[tp, rows_of(there)],
@@ -321,59 +320,30 @@
             device_id_type=MESH,
         )
 
-    def chunk_span(c):
-        first, size = c
-        start = flipped(ep // size, first // size, n // size) * size * capacity
-        return pl.ds(pl.multiple_of(start, size * capacity), size * capacity)
-
-    def half_rows_of(index):
-        return rows_of(index % near)
-
-    def half_span(c):
-        first, size = c
-        start = (flipped(ep // size, first // size, n // size) % (near // size)) * size * capacity
-        return pl.ds(pl.multiple_of(start, size * capacity), size * capacity)
-
-    def partial_copy(j):
-        block = half_rows_of(flipped(ep, j, n))
+    def partial_copy(k):
+        j, there = partner(k)
         return pltpu.make_async_remote_copy(
-            src_ref=part_send.at[block],
-            dst_ref=part_recv.at[block],
+            src_ref=part_send.at[rows_of(there)],
+            dst_ref=part_recv.at[rows_of(there)],
             send_sem=part_ssem.at[j],
             recv_sem=part_rsem.at[j],
             device_id=(ep, other),
             device_id_type=MESH,
         )
 
-    def give_back(j):
-        there = flipped(ep, j, n)
-        if j < near:
-            src, dst = near_part.at[:, half_rows_of(there)], near_back.at[:, half_rows_of(ep)]
-        else:
-            src, dst = result.at[half_rows_of(there)], returned.at[half_rows_of(ep)]
+    def give_back(k):
+        j, there = partner(k)
         return pltpu.make_async_remote_copy(
-            src_ref=src,
-            dst_ref=dst,
+            src_ref=result.at[rows_of(there)],
+            dst_ref=returned.at[own_rows],
             send_sem=ret_send.at[j],
             recv_sem=ret_recv.at[j],
             device_id=(there, tp),
             device_id_type=MESH,
         )
 
-    near_copy = pltpu.make_async_remote_copy(
-        src_ref=near_send,
-        dst_ref=near_recv,
-        send_sem=near_sem.at[0],
-        recv_sem=near_sem.at[1],
-        device_id=(ep, other),
-        device_id_type=MESH,
-    )
-
-    def members(c):
-        return [j for j in range(c[0], c[0] + c[1]) if j]
-
-    for j in range(1, n):
-        dispatch(j).start()
+    for k in range(1, n):
+        dispatch(k).start()
     arrived[:, own_rows] = outgoing[:, own_rows]
 
     def contract(left, right):
@@ -396,8 +366,7 @@
         (share * value).astype(jnp.bfloat16).astype(jnp.float32) for value in (first, 1.0 - first)
     ]
     spread = jnp.where(chosen[0], weights[0], 0.0) + jnp.where(chosen[1], weights[1], 0.0)
-    for part in range(2):
-        combine_w[part] = spread[part * far_rows : (part + 1) * far_rows].T.astype(jnp.bfloat16)
+    combine_w[...] = spread.T.astype(jnp.bfloat16)
 
     def mixer():
         halo_copy.wait()
@@ -431,8 +400,12 @@
                 grouped_v[...], out_w[:, lanes], preferred_element_type=jnp.float32
             ).astype(jnp.bfloat16)
 
-    def expert(c):
-        span = chunk_span(c)
+    groups = [list(range(first, first + CHUNK)) for first in range(0, n, CHUNK)]
+
+    def expert(group):
+        size = len(group)
+        start = partner(group[0])[1] // size * (size * capacity)
+        span = pl.ds(pl.multiple_of(start, size * capacity), size * capacity)
         sums = []
         for weight in (gate_w, up_w):
             sums.append(
@@ -446,83 +419,89 @@
                 hidden, down_w[index], preferred_element_type=jnp.float32
             ).astype(jnp.bfloat16)
 
-        span = half_span(c)
-        if c[0] < near:
-            near_part[0, span] = part(0)
-            near_part[1, span] = part(1)
-            for j in members(c):
-                give_back(j).start()
-            if c[0] == 0:
-                block = half_rows_of(ep)
-                near_back[:, block] = near_part[:, block]
-        else:
-            part_send[span] = part(other)
-            for j in members(c):
-                partial_copy(j).start()
-            part_own[span] = part(tp)
-
-    def finish(c):
-        for j in members(c):
-            finish_one(j)
-
-    def finish_one(j):
-        block = half_rows_of(flipped(ep, j, n))
-        partial_copy(j).wait_recv()
-        result[block] = (
+        part_send[span] = part(other)
+        for k in group:
+            partial_copy(k).start()
+        part_own[span] = part(tp)
+
+    def finish(k):
+        block = rows_of(partner(k)[1])
+        partial_copy(k).wait_recv()
+        total = (
             part_own[block].astype(jnp.float32) + part_recv[block].astype(jnp.float32)
         ).astype(jnp.bfloat16)
-        give_back(j).start()
-
-    def arrive(c):
-        for j in members(c):
-            dispatch(j).wait_recv()
-            if j >= near:
-                swap(j).start()
-
-    def swapped(c):
-        for j in members(c):
-            swap(j).wait_recv()
-
-    mixer()
+        if k == 0:
+            returned[block] = total
+        else:
+            result[block] = total
+            give_back(k).start()
+
+    def pass_on(k):
+        dispatch(k).wait_recv()
+        swap(k).start()
+
+    own, beside, far, last = groups
+    early, late = own[:2], own[2:]
+
+    def late_plane():
+        for k in late:
+            dispatch(k).wait_recv()
+        expert(late)
+
+    def late_back():
+        for k in late:
+            finish(k)
+
     for index in (0, 1, 3, 4):
         loads[index].wait()
-    for c in near_chunks:
-        arrive(c)
-        expert(c)
-    unfinished = []
-    for c in far_chunks:
-        for j in members(c):
-            dispatch(j).wait_recv()
-            swap(j).start()
-            if unfinished:
-                finish_one(unfinished.pop(0))
-        swapped(c)
-        expert(c)
-        unfinished += members(c)
-    for j in unfinished:
-        finish_one(j)
-    for j in range(1, near):
-        give_back(j).wait_recv()
-    near_send[...] = jnp.dot(
-        combine_w[side], near_back[other], preferred_element_type=jnp.float32
+    dispatch(1).wait_recv()
+    expert(early)
+    mixer()
+    pl.when(inner == 0)(late_plane)
+    for k in far:
+        pass_on(k)
+    for k in early:
+        finish(k)
+    pl.when(inner == 0)(late_back)
+    for pair in (far[:2], far[2:]):
+        for k in pair:
+            swap(k).wait_recv()
+        expert(pair)
+    for pair in (beside[:2], beside[2:]):
+        for k in pair:
+            dispatch(k).wait_recv()
+        expert(pair)
+    for k, earlier_k in zip(last, far):
+        pass_on(k)
+        finish(earlier_k)
+    for k in beside:
+        finish(k)
+    for pair in (last[:2], last[2:]):
+        for k in pair:
+            swap(k).wait_recv()
+        expert(pair)
+    pl.when(inner == 1)(late_plane)
+    for k in last:
+        finish(k)
+    pl.when(inner == 1)(late_back)
+    for k in far:
+        give_back(k).wait_recv()
+    for k in beside:
+        give_back(k).wait_recv()
+    for k in last:
+        give_back(k).wait_recv()
+    for k in own[1:]:
+        give_back(k).wait_recv()
+    moe_out_ref[...] = jnp.dot(
+        combine_w[...], returned[...], preferred_element_type=jnp.float32
     ).astype(jnp.bfloat16)
-    near_copy.start()
-    near_own[...] = jnp.dot(combine_w[side], near_back[tp], preferred_element_type=jnp.float32)
-    near_copy.wait_recv()
-    near_own[...] += near_recv[...].astype(jnp.float32)
-    for j in range(near, n):
-        give_back(j).wait_recv()
-    moe_out_ref[...] = (
-        near_own[...]
-        + jnp.dot(combine_w[1 - side], returned[...], preferred_element_type=jnp.float32)
-    ).astype(jnp.bfloat16)
-    near_copy.wait_send()
-    for j in range(1, n):
-        dispatch(j).wait_send()
-        give_back(j).wait_send()
-        if j >= near:
-            swap(j).wait_send()
-            partial_copy(j).wait_send()
+    partial_copy(0).wait_send()
+    for k in range(1, n):
+        dispatch(k).wait_send()
+        give_back(k).wait_send()
+        partial_copy(k).wait_send()
+        if k >= near:
+            swap(k).wait_send()
 
 
 def fused(
@@ -548,7 +527,6 @@
     half = width // 2
     slots = n * capacity
     hidden = gate_weight.shape[2]
-    far_rows = slots // 2
     bf16 = jnp.bfloat16
     vmem = pl.BlockSpec(memory_space=pltpu.VMEM)
     hbm = pl.BlockSpec(memory_space=pl.ANY)
@@ -574,17 +552,12 @@
             pltpu.VMEM((tokens, width), bf16),
             pltpu.VMEM((2, slots, half), bf16),
             pltpu.VMEM((2, slots, half), bf16),
-            pltpu.VMEM((far_rows, half), bf16),
-            pltpu.VMEM((far_rows, half), bf16),
-            pltpu.VMEM((far_rows, half), bf16),
-            pltpu.VMEM((far_rows, half), bf16),
-            pltpu.VMEM((far_rows, half), bf16),
-            pltpu.VMEM((2, far_rows, half), bf16),
-            pltpu.VMEM((2, far_rows, half), bf16),
-            pltpu.VMEM((tokens, half), jnp.float32),
-            pltpu.VMEM((tokens, half), bf16),
-            pltpu.VMEM((tokens, half), bf16),
-            pltpu.VMEM((2, tokens, far_rows), bf16),
+            pltpu.VMEM((slots, half), bf16),
+            pltpu.VMEM((slots, half), bf16),
+            pltpu.VMEM((slots, half), bf16),
+            pltpu.VMEM((slots, half), bf16),
+            pltpu.VMEM((slots, half), bf16),
+            pltpu.VMEM((tokens, slots), bf16),
             dma((5,)),
             dma((2,)),
             dma((n,)),
@@ -595,7 +568,6 @@
             dma((n,)),
             dma((n,)),
             dma((n,)),
-            dma((2,)),
         ],
         compiler_params=pltpu.CompilerParams(
             collective_id=0, has_side_effects=True, vmem_limit_bytes=60 * 1024 * 1024
@@ -624,8 +596,7 @@
     fits = (
         n_tp == 2
         and inner_pick.shape[1] == 2
-        and n & (n - 1) == 0
-        and n >= 2 * CHUNK
+        and n == 4 * CHUNK
         and inner_router.shape[1] == n
         and capacity % 16 == 0
         and mix_input.shape[0] >= LEAD

time: 66.7 us -> 59.5 us (0.89)
  Pallas kernels: 64.2 us -> 56.8 us
    pallas_call x1, Pallas kernels: 64.2 us -> 56.8 us  [fused(): pl.pallas_call(functools.partial(fused_kernel, n, capacity, expert_count...]
where the time goes in v1:
time: 59.5 us; the launch traced here: 59.1 us
  Pallas kernels  56.8 us (95%)
  local copies, waits for them, and re-layouts  1.67 us (3%)
  between operations  0.64 us (1%)
    pallas_call x1, Pallas kernels, fused(): pl.pallas_call(functools.partial(fused_kernel, n, capacity, expert_count...  56.8 us
    unnamed x2, local copies, waits for them, and re-layouts  1.67 us

profile of v1, /device:TPU:0, one launch (start us, length us, event | category | flops | bytes accessed | tf_op | source)
XLA Modules:
  0.0 59.1 jit_solution(7260266802349413962)
XLA Ops:
  0.6 56.8 %shard_map.140 = (bf16[256,2048]{1,0:T(8,128)(2,1)S(1)}, bf16[128,1024]{1,0:T(8,128)(2,1)S(1)}) custom-call(bf16[256,1024]{1,0:T(8,128)(2,1)} %mix_ref.1, bf16[8,128,128]{2,1,0:T(8,128)(2,1)} %pool_w_ref.1, f32[1,1024]{1,0:T(1,128)} %bitcast.9, bf16[1024,2048]{1,0:T(8,128)(2,1)} %out_w_hbm.1, bf16[128,2048]{1,0:T(8,128)(2,1)} %moe_ref.1, f32[1,2048]{1,0:T(1,128)} %bitcast.8, ...), custom_call_target="tpu_custom_call" | custom-call | tf_op jit(solution)/shard_map/pallas_call | solution.py:534
  57.4 1.0 %copy.17 = bf16[256,2048]{1,0:T(8,128)(2,1)} copy(bf16[256,2048]{1,0:T(8,128)(2,1)S(1)} %get-tuple-element.2) | data formatting | bytes 2097152
  58.4 0.7 %copy.18 = bf16[128,1024]{1,0:T(8,128)(2,1)} copy(bf16[128,1024]{1,0:T(8,128)(2,1)S(1)} %get-tuple-element.3) | data formatting | bytes 524288

commit v2 on v1

--- a/solution.py
+++ b/solution.py
@@ -200,6 +200,10 @@
     result,
     returned,
     combine_w,
+    slot_info,
+    raw_info,
+    raw_rows,
+    relayed,
     load_sem,
     halo_sem,
     send_sem,
@@ -210,6 +214,8 @@
     part_rsem,
     ret_send,
     ret_recv,
+    raw_sem,
+    relay_send,
 ):
     ep, tp = lax.axis_index("ep"), lax.axis_index("tp")
     other = 1 - tp
@@ -246,7 +252,8 @@
         jnp.maximum(jnp.sum(values * values, axis=1, keepdims=True) * (1.0 / width), NORM_FLOOR)
     )
     normed = (values * scale * gain_ref[...]).astype(jnp.bfloat16)
-    normed_v[...] = normed
+    for part in range(2):
+        normed_v[part] = normed[:, part * half : (part + 1) * half]
 
     group_pick = gp_ref[...]
     expert_count = inner_rt_ref.shape[0]
@@ -268,8 +275,10 @@
     pick = jnp.where(chosen[0] | chosen[1], 1.0, 0.0).astype(jnp.bfloat16)
     for part in range(2):
         outgoing[part] = jnp.dot(
-            pick, normed_v[:, part * half : (part + 1) * half], preferred_element_type=jnp.float32
+            pick, normed_v[part], preferred_element_type=jnp.float32
         ).astype(jnp.bfloat16)
+    for k in range(2):
+        slot_info[k : k + 1, :] = slot_of[k]
 
     pl.semaphore_wait(barrier, len(greeted))
 
@@ -283,6 +292,8 @@
         device_id_type=MESH,
     )
     halo_copy.start()
+
+    relay_lanes = [slice(first, first + half // 2) for first in range(0, half, half // 2)]
 
     def rows_of(index):
         return pl.ds(pl.multiple_of(index * capacity, capacity), capacity)
@@ -342,8 +353,73 @@
             device_id_type=MESH,
         )
 
-    for k in range(1, n):
+    raw_copies = [
+        pltpu.make_async_remote_copy(
+            src_ref=src,
+            dst_ref=dst,
+            send_sem=raw_sem.at[0, index],
+            recv_sem=raw_sem.at[1, index],
+            device_id=(flipped(ep, near, n), tp),
+            device_id_type=MESH,
+        )
+        for index, (src, dst) in enumerate(
+            [(slot_info, raw_info)]
+            + [(normed_v.at[tp, :, lanes], raw_rows.at[:, lanes]) for lanes in relay_lanes]
+        )
+    ]
+
+    def relay_copy(m, lanes, index):
+        there = flipped(ep, m, n)
+        return pltpu.make_async_remote_copy(
+            src_ref=relayed.at[rows_of(there % near), lanes],
+            dst_ref=arrived.at[tp, rows_of(flipped(ep, near, n)), lanes],
+            send_sem=relay_send.at[index, m],
+            recv_sem=recv_sem.at[near + m],
+            device_id=(there, tp),
+            device_id_type=MESH,
+        )
+
+    relay_order = list(range(CHUNK, near)) + list(range(1, CHUNK))
+
+    def relay():
+        raw_copies[0].wait_recv()
+        first_slot = (ep // near) * (near * capacity)
+        half_ids = lax.broadcasted_iota(jnp.int32, (near * capacity, tokens), 0) + first_slot
+        half_pick = jnp.where(
+            (half_ids == raw_info[0:1, :]) | (half_ids == raw_info[1:2, :]), 1.0, 0.0
+        ).astype(jnp.bfloat16)
+        for index, lanes in enumerate(relay_lanes):
+            raw_copies[1 + index].wait_recv()
+            relayed[:, lanes] = jnp.dot(
+                half_pick, raw_rows[:, lanes], preferred_element_type=jnp.float32
+            ).astype(jnp.bfloat16)
+            for m in relay_order:
+                relay_copy(m, lanes, index).start()
+            arrived[tp, rows_of(flipped(ep, near, n)), lanes] = relayed[rows_of(ep % near), lanes]
+
+    def sends_outer():
+        for copy in raw_copies:
+            copy.start()
+
+    def sends_inner():
+        for k in range(near, n):
+            dispatch(k).start()
+
+    def sent_outer():
+        for copy in raw_copies:
+            copy.wait_send()
+
+    def sent_inner():
+        for k in range(near, n):
+            dispatch(k).wait_send()
+        for index, lanes in enumerate(relay_lanes):
+            for m in relay_order:
+                relay_copy(m, lanes, index).wait_send()
+
+    for k in range(1, near):
         dispatch(k).start()
+    pl.when(inner == 0)(sends_outer)
+    pl.when(inner == 1)(sends_inner)
     arrived[:, own_rows] = outgoing[:, own_rows]
 
     def contract(left, right):
@@ -351,8 +427,11 @@
             left, right, (((1,), (1,)), ((), ())), preferred_element_type=jnp.float32
         )
 
-    group_logits = contract(group_rt_ref[...], normed_v[...])
-    inner_logits = contract(inner_rt_ref[...], normed_v[...])
+    def logits_of(router):
+        return contract(router[:, :half], normed_v[0]) + contract(router[:, half:], normed_v[1])
+
+    group_logits = logits_of(group_rt_ref)
+    inner_logits = logits_of(inner_rt_ref)
     group_ids = lax.broadcasted_iota(jnp.int32, group_logits.shape, 0)
     own_logit = jnp.sum(
         jnp.where(group_ids == group_pick, group_logits, 0.0), axis=0, keepdims=True
@@ -437,7 +516,10 @@
             give_back(k).start()
 
     def pass_on(k):
-        dispatch(k).wait_recv()
+        if k == near + CHUNK:
+            pl.when(inner == 0)(dispatch(k).wait_recv)
+        else:
+            dispatch(k).wait_recv()
         swap(k).start()
 
     own, beside, far, last = groups
@@ -471,9 +553,11 @@
         for k in pair:
             dispatch(k).wait_recv()
         expert(pair)
-    for k, earlier_k in zip(last, far):
+    for k in far:
+        finish(k)
+    pl.when(inner == 1)(relay)
+    for k in last:
         pass_on(k)
-        finish(earlier_k)
     for k in beside:
         finish(k)
     for pair in (last[:2], last[2:]):
@@ -496,8 +580,11 @@
         combine_w[...], returned[...], preferred_element_type=jnp.float32
     ).astype(jnp.bfloat16)
     partial_copy(0).wait_send()
+    pl.when(inner == 0)(sent_outer)
+    pl.when(inner == 1)(sent_inner)
     for k in range(1, n):
-        dispatch(k).wait_send()
+        if k < near:
+            dispatch(k).wait_send()
         give_back(k).wait_send()
         partial_copy(k).wait_send()
         if k >= near:
@@ -549,7 +636,7 @@
             pltpu.VMEM((LEAD, channels), bf16),
             pltpu.VMEM((rows, channels), bf16),
             pltpu.VMEM((rows, channels), bf16),
-            pltpu.VMEM((tokens, width), bf16),
+            pltpu.VMEM((2, tokens, half), bf16),
             pltpu.VMEM((2, slots, half), bf16),
             pltpu.VMEM((2, slots, half), bf16),
             pltpu.VMEM((slots, half), bf16),
@@ -558,6 +645,10 @@
             pltpu.VMEM((slots, half), bf16),
             pltpu.VMEM((slots, half), bf16),
             pltpu.VMEM((tokens, slots), bf16),
+            pltpu.VMEM((2, tokens), jnp.int32),
+            pltpu.VMEM((2, tokens), jnp.int32),
+            pltpu.VMEM((tokens, half), bf16),
+            pltpu.VMEM((slots // 2, half), bf16),
             dma((5,)),
             dma((2,)),
             dma((n,)),
@@ -568,6 +659,8 @@
             dma((n,)),
             dma((n,)),
             dma((n,)),
+            dma((2, 3)),
+            dma((2, n // 2)),
         ],
         compiler_params=pltpu.CompilerParams(
             collective_id=0, has_side_effects=True, vmem_limit_bytes=60 * 1024 * 1024

time: 59.5 us -> 57.6 us (0.968)
  Pallas kernels: 56.8 us -> 54.6 us
    pallas_call x1, Pallas kernels: 56.8 us -> 54.6 us  [fused(): pl.pallas_call(functools.partial(fused_kernel, n, capacity, expert_count...]
where the time goes in v2:
time: 57.6 us; the launch traced here: 56.9 us
  Pallas kernels  54.6 us (95%)
  local copies, waits for them, and re-layouts  1.67 us (3%)
  between operations  0.64 us (1%)
    pallas_call x1, Pallas kernels, fused(): pl.pallas_call(functools.partial(fused_kernel, n, capacity, expert_count...  54.6 us
    unnamed x2, local copies, waits for them, and re-layouts  1.67 us

profile of v2, /device:TPU:0, one launch (start us, length us, event | category | flops | bytes accessed | tf_op | source)
XLA Modules:
  0.0 56.9 jit_solution(16574575928848248332)
XLA Ops:
  0.6 54.6 %shard_map.140 = (bf16[256,2048]{1,0:T(8,128)(2,1)S(1)}, bf16[128,1024]{1,0:T(8,128)(2,1)S(1)}) custom-call(bf16[256,1024]{1,0:T(8,128)(2,1)} %mix_ref.1, bf16[8,128,128]{2,1,0:T(8,128)(2,1)} %pool_w_ref.1, f32[1,1024]{1,0:T(1,128)} %bitcast.9, bf16[1024,2048]{1,0:T(8,128)(2,1)} %out_w_hbm.1, bf16[128,2048]{1,0:T(8,128)(2,1)} %moe_ref.1, f32[1,2048]{1,0:T(1,128)} %bitcast.8, ...), custom_call_target="tpu_custom_call" | custom-call | tf_op jit(solution)/shard_map/pallas_call | solution.py:621
  55.2 1.0 %copy.17 = bf16[256,2048]{1,0:T(8,128)(2,1)} copy(bf16[256,2048]{1,0:T(8,128)(2,1)S(1)} %get-tuple-element.2) | data formatting | bytes 2097152
  56.2 0.7 %copy.18 = bf16[128,1024]{1,0:T(8,128)(2,1)} copy(bf16[128,1024]{1,0:T(8,128)(2,1)S(1)} %get-tuple-element.3) | data formatting | bytes 524288

commit v3 on v2

--- a/solution.py
+++ b/solution.py
@@ -206,16 +206,12 @@
     relayed,
     load_sem,
     halo_sem,
-    send_sem,
+    sent_sem,
     recv_sem,
-    swap_send,
     swap_recv,
-    part_ssem,
-    part_rsem,
-    ret_send,
+    part_recv_sem,
     ret_recv,
     raw_sem,
-    relay_send,
 ):
     ep, tp = lax.axis_index("ep"), lax.axis_index("tp")
     other = 1 - tp
@@ -305,78 +301,74 @@
         shift = CHUNK if k < near + CHUNK else -CHUNK
         return k + inner * shift, there + inner * (CHUNK - 2 * CHUNK * ((there // CHUNK) % 2))
 
+    def pair_rows(k):
+        start = partner(k)[1] // 2 * (2 * capacity)
+        return pl.ds(pl.multiple_of(start, 2 * capacity), 2 * capacity)
+
+    def remote(src, dst, sent, received, device):
+        return pltpu.make_async_remote_copy(
+            src_ref=src,
+            dst_ref=dst,
+            send_sem=sent,
+            recv_sem=received,
+            device_id=device,
+            device_id_type=MESH,
+        )
+
+    def landed(ref, semaphore):
+        remote(ref, ref, sent_sem.at[0], semaphore, (ep, other)).wait_recv()
+
+    def all_sent(ref, semaphore):
+        remote(ref, ref, semaphore, ret_recv.at[0], (ep, other)).wait_send()
+
     def dispatch(k):
         j, there = partner(k)
         if k < near:
             src, dst = outgoing.at[:, rows_of(there)], arrived.at[:, own_rows]
+            sent, received = sent_sem.at[0], recv_sem.at[k // 2]
         else:
             src, dst = outgoing.at[tp, rows_of(there)], arrived.at[tp, own_rows]
-        return pltpu.make_async_remote_copy(
-            src_ref=src,
-            dst_ref=dst,
-            send_sem=send_sem.at[j],
-            recv_sem=recv_sem.at[j],
-            device_id=(there, tp),
-            device_id_type=MESH,
+            sent, received = sent_sem.at[1], recv_sem.at[near // 2 + j - near]
+        return remote(src, dst, sent, received, (there, tp))
+
+    def swap(k):
+        block = arrived.at[tp, rows_of(partner(k)[1])]
+        received = swap_recv.at[(k - near) // 2]
+        return remote(block, block, sent_sem.at[2], received, (ep, other))
+
+    def partial_copy(k):
+        block = rows_of(partner(k)[1])
+        received = part_recv_sem.at[k // 2 if k < near + CHUNK else k - near // 2 - CHUNK // 2]
+        return remote(
+            part_send.at[block], part_recv.at[block], sent_sem.at[3], received, (ep, other)
         )
 
-    def swap(k):
-        j, there = partner(k)
-        return pltpu.make_async_remote_copy(
-            src_ref=arrived.at[tp, rows_of(there)],
-            dst_ref=arrived.at[tp, rows_of(there)],
-            send_sem=swap_send.at[j],
-            recv_sem=swap_recv.at[j],
-            device_id=(ep, other),
-            device_id_type=MESH,
+    def give_back(k):
+        there = partner(k)[1]
+        return remote(
+            result.at[rows_of(there)],
+            returned.at[own_rows],
+            sent_sem.at[4],
+            ret_recv.at[0],
+            (there, tp),
         )
 
-    def partial_copy(k):
-        j, there = partner(k)
-        return pltpu.make_async_remote_copy(
-            src_ref=part_send.at[rows_of(there)],
-            dst_ref=part_recv.at[rows_of(there)],
-            send_sem=part_ssem.at[j],
-            recv_sem=part_rsem.at[j],
-            device_id=(ep, other),
-            device_id_type=MESH,
-        )
-
-    def give_back(k):
-        j, there = partner(k)
-        return pltpu.make_async_remote_copy(
-            src_ref=result.at[rows_of(there)],
-            dst_ref=returned.at[own_rows],
-            send_sem=ret_send.at[j],
-            recv_sem=ret_recv.at[j],
-            device_id=(there, tp),
-            device_id_type=MESH,
-        )
-
     raw_copies = [
-        pltpu.make_async_remote_copy(
-            src_ref=src,
-            dst_ref=dst,
-            send_sem=raw_sem.at[0, index],
-            recv_sem=raw_sem.at[1, index],
-            device_id=(flipped(ep, near, n), tp),
-            device_id_type=MESH,
-        )
+        remote(src, dst, raw_sem.at[min(index, 1)], raw_sem.at[2 + index], (flipped(ep, near, n), tp))
         for index, (src, dst) in enumerate(
             [(slot_info, raw_info)]
             + [(normed_v.at[tp, :, lanes], raw_rows.at[:, lanes]) for lanes in relay_lanes]
         )
     ]
 
-    def relay_copy(m, lanes, index):
+    def relay_copy(m, lanes):
         there = flipped(ep, m, n)
-        return pltpu.make_async_remote_copy(
-            src_ref=relayed.at[rows_of(there % near), lanes],
-            dst_ref=arrived.at[tp, rows_of(flipped(ep, near, n)), lanes],
-            send_sem=relay_send.at[index, m],
-            recv_sem=recv_sem.at[near + m],
-            device_id=(there, tp),
-            device_id_type=MESH,
+        return remote(
+            relayed.at[rows_of(there % near), lanes],
+            arrived.at[tp, rows_of(flipped(ep, near, n)), lanes],
+            sent_sem.at[5],
+            recv_sem.at[near // 2 + m],
+            (there, tp),
         )
 
     relay_order = list(range(CHUNK, near)) + list(range(1, CHUNK))
@@ -394,7 +386,7 @@
                 half_pick, raw_rows[:, lanes], preferred_element_type=jnp.float32
             ).astype(jnp.bfloat16)
             for m in relay_order:
-                relay_copy(m, lanes, index).start()
+                relay_copy(m, lanes).start()
             arrived[tp, rows_of(flipped(ep, near, n)), lanes] = relayed[rows_of(ep % near), lanes]
 
     def sends_outer():
@@ -406,15 +398,12 @@
             dispatch(k).start()
 
     def sent_outer():
-        for copy in raw_copies:
-            copy.wait_send()
+        raw_copies[0].wait_send()
+        all_sent(normed_v.at[tp], raw_sem.at[1])
 
     def sent_inner():
-        for k in range(near, n):
-            dispatch(k).wait_send()
-        for index, lanes in enumerate(relay_lanes):
-            for m in relay_order:
-                relay_copy(m, lanes, index).wait_send()
+        all_sent(outgoing.at[0, pl.ds(0, near * capacity)], sent_sem.at[1])
+        all_sent(relayed.at[pl.ds(0, (near - 1) * capacity)], sent_sem.at[5])
 
     for k in range(1, near):
         dispatch(k).start()
@@ -503,17 +492,25 @@
             partial_copy(k).start()
         part_own[span] = part(tp)
 
-    def finish(k):
-        block = rows_of(partner(k)[1])
-        partial_copy(k).wait_recv()
-        total = (
+    def add_up(block):
+        result[block] = (
             part_own[block].astype(jnp.float32) + part_recv[block].astype(jnp.float32)
         ).astype(jnp.bfloat16)
-        if k == 0:
-            returned[block] = total
-        else:
-            result[block] = total
-            give_back(k).start()
+
+    def finish_one(k):
+        partial_copy(k).wait_recv()
+        add_up(rows_of(partner(k)[1]))
+        give_back(k).start()
+
+    def finish(pair):
+        block = pair_rows(pair[0])
+        landed(part_recv.at[block], part_recv_sem.at[pair[0] // 2])
+        add_up(block)
+        for k in pair:
+            if k:
+                give_back(k).start()
+        if pair[0] == 0:
+            returned[own_rows] = result[own_rows]
 
     def pass_on(k):
         if k == near + CHUNK:
@@ -522,73 +519,63 @@
             dispatch(k).wait_recv()
         swap(k).start()
 
-    own, beside, far, last = groups
-    early, late = own[:2], own[2:]
+    def straight(pair):
+        if pair[0] == 0:
+            dispatch(1).wait_recv()
+        else:
+            landed(arrived.at[:, pair_rows(pair[0])], recv_sem.at[pair[0] // 2])
+        expert(pair)
+
+    def swapped(pair):
+        landed(arrived.at[other, pair_rows(pair[0])], swap_recv.at[(pair[0] - near) // 2])
+        expert(pair)
+
+    early, late, beside, beyond, far, farther, last, latest = [
+        [first, first + 1] for first in range(0, n, 2)
+    ]
 
     def late_plane():
-        for k in late:
-            dispatch(k).wait_recv()
-        expert(late)
+        straight(late)
 
     def late_back():
-        for k in late:
-            finish(k)
+        finish(late)
 
     for index in (0, 1, 3, 4):
         loads[index].wait()
-    dispatch(1).wait_recv()
-    expert(early)
+    straight(early)
     mixer()
     pl.when(inner == 0)(late_plane)
-    for k in far:
+    for k in far + farther:
         pass_on(k)
-    for k in early:
-        finish(k)
+    finish(early)
     pl.when(inner == 0)(late_back)
-    for pair in (far[:2], far[2:]):
-        for k in pair:
-            swap(k).wait_recv()
-        expert(pair)
-    for pair in (beside[:2], beside[2:]):
-        for k in pair:
-            dispatch(k).wait_recv()
-        expert(pair)
-    for k in far:
-        finish(k)
+    swapped(far)
+    swapped(farther)
+    straight(beside)
+    straight(beyond)
+    finish(far)
     pl.when(inner == 1)(relay)
-    for k in last:
+    finish(farther)
+    for k in last + latest:
         pass_on(k)
-    for k in beside:
-        finish(k)
-    for pair in (last[:2], last[2:]):
-        for k in pair:
-            swap(k).wait_recv()
-        expert(pair)
+    finish(beside)
+    finish(beyond)
+    swapped(last)
+    swapped(latest)
     pl.when(inner == 1)(late_plane)
-    for k in last:
-        finish(k)
+    for k in last + latest:
+        finish_one(k)
     pl.when(inner == 1)(late_back)
-    for k in far:
-        give_back(k).wait_recv()
-    for k in beside:
-        give_back(k).wait_recv()
-    for k in last:
-        give_back(k).wait_recv()
-    for k in own[1:]:
-        give_back(k).wait_recv()
+    landed(returned.at[pl.ds(0, (n - 1) * capacity)], ret_recv.at[0])
     moe_out_ref[...] = jnp.dot(
         combine_w[...], returned[...], preferred_element_type=jnp.float32
     ).astype(jnp.bfloat16)
-    partial_copy(0).wait_send()
     pl.when(inner == 0)(sent_outer)
     pl.when(inner == 1)(sent_inner)
-    for k in range(1, n):
-        if k < near:
-            dispatch(k).wait_send()
-        give_back(k).wait_send()
-        partial_copy(k).wait_send()
-        if k >= near:
-            swap(k).wait_send()
+    all_sent(outgoing.at[:, pl.ds(0, (near - 1) * capacity)], sent_sem.at[0])
+    all_sent(arrived.at[0, pl.ds(0, near * capacity)], sent_sem.at[2])
+    all_sent(part_send, sent_sem.at[3])
+    all_sent(result.at[pl.ds(0, (n - 1) * capacity)], sent_sem.at[4])
 
 
 def fused(
@@ -651,16 +638,12 @@
             pltpu.VMEM((slots // 2, half), bf16),
             dma((5,)),
             dma((2,)),
-            dma((n,)),
-            dma((n,)),
-            dma((n,)),
-            dma((n,)),
-            dma((n,)),
-            dma((n,)),
-            dma((n,)),
-            dma((n,)),
-            dma((2, 3)),
-            dma((2, n // 2)),
+            dma((6,)),
+            dma((n // 2 + n // 4,)),
+            dma((n // 4,)),
+            dma((n // 2 + n // 8,)),
+            dma((1,)),
+            dma((5,)),
         ],
         compiler_params=pltpu.CompilerParams(
             collective_id=0, has_side_effects=True, vmem_limit_bytes=60 * 1024 * 1024

time: 57.6 us -> 56.1 us (0.974)
  Pallas kernels: 54.6 us -> 53.5 us
    pallas_call x1, Pallas kernels: 54.6 us -> 53.5 us  [fused(): pl.pallas_call(functools.partial(fused_kernel, n, capacity, expert_count...]
where the time goes in v3:
time: 56.1 us; the launch traced here: 55.8 us
  Pallas kernels  53.5 us (95%)
  local copies, waits for them, and re-layouts  1.67 us (3%)
  between operations  0.64 us (1%)
    pallas_call x1, Pallas kernels, fused(): pl.pallas_call(functools.partial(fused_kernel, n, capacity, expert_count...  53.5 us
    unnamed x2, local copies, waits for them, and re-layouts  1.67 us

profile of v3, /device:TPU:0, one launch (start us, length us, event | category | flops | bytes accessed | tf_op | source)
XLA Modules:
  0.0 55.8 jit_solution(13239455561455955705)
XLA Ops:
  0.6 53.5 %shard_map.140 = (bf16[256,2048]{1,0:T(8,128)(2,1)S(1)}, bf16[128,1024]{1,0:T(8,128)(2,1)S(1)}) custom-call(bf16[256,1024]{1,0:T(8,128)(2,1)} %mix_ref.1, bf16[8,128,128]{2,1,0:T(8,128)(2,1)} %pool_w_ref.1, f32[1,1024]{1,0:T(1,128)} %bitcast.9, bf16[1024,2048]{1,0:T(8,128)(2,1)} %out_w_hbm.1, bf16[128,2048]{1,0:T(8,128)(2,1)} %moe_ref.1, f32[1,2048]{1,0:T(1,128)} %bitcast.8, ...), custom_call_target="tpu_custom_call" | custom-call | tf_op jit(solution)/shard_map/pallas_call | solution.py:608
  54.1 1.0 %copy.17 = bf16[256,2048]{1,0:T(8,128)(2,1)} copy(bf16[256,2048]{1,0:T(8,128)(2,1)S(1)} %get-tuple-element.2) | data formatting | bytes 2097152
  55.1 0.7 %copy.18 = bf16[128,1024]{1,0:T(8,128)(2,1)} copy(bf16[128,1024]{1,0:T(8,128)(2,1)S(1)} %get-tuple-element.3) | data formatting | bytes 524288

commit v4 on v3

--- a/solution.py
+++ b/solution.py
@@ -325,7 +325,7 @@
         j, there = partner(k)
         if k < near:
             src, dst = outgoing.at[:, rows_of(there)], arrived.at[:, own_rows]
-            sent, received = sent_sem.at[0], recv_sem.at[k // 2]
+            sent, received = sent_sem.at[0], recv_sem.at[near // 2 + near if k == 2 else k // 2]
         else:
             src, dst = outgoing.at[tp, rows_of(there)], arrived.at[tp, own_rows]
             sent, received = sent_sem.at[1], recv_sem.at[near // 2 + j - near]
@@ -338,7 +338,7 @@
 
     def partial_copy(k):
         block = rows_of(partner(k)[1])
-        received = part_recv_sem.at[k // 2 if k < near + CHUNK else k - near // 2 - CHUNK // 2]
+        received = part_recv_sem.at[k]
         return remote(
             part_send.at[block], part_recv.at[block], sent_sem.at[3], received, (ep, other)
         )
@@ -492,25 +492,17 @@
             partial_copy(k).start()
         part_own[span] = part(tp)
 
-    def add_up(block):
-        result[block] = (
-            part_own[block].astype(jnp.float32) + part_recv[block].astype(jnp.float32)
-        ).astype(jnp.bfloat16)
-
-    def finish_one(k):
-        partial_copy(k).wait_recv()
-        add_up(rows_of(partner(k)[1]))
-        give_back(k).start()
-
-    def finish(pair):
-        block = pair_rows(pair[0])
-        landed(part_recv.at[block], part_recv_sem.at[pair[0] // 2])
-        add_up(block)
-        for k in pair:
+    def finish(ks):
+        for k in ks:
+            block = rows_of(partner(k)[1])
+            partial_copy(k).wait_recv()
+            result[block] = (
+                part_own[block].astype(jnp.float32) + part_recv[block].astype(jnp.float32)
+            ).astype(jnp.bfloat16)
             if k:
                 give_back(k).start()
-        if pair[0] == 0:
-            returned[own_rows] = result[own_rows]
+            else:
+                returned[block] = result[block]
 
     def pass_on(k):
         if k == near + CHUNK:
@@ -535,7 +527,15 @@
     ]
 
     def late_plane():
-        straight(late)
+        for k in late:
+            dispatch(k).wait_recv()
+            expert([k])
+
+    def beyond_plane():
+        straight(beyond)
+
+    def beyond_back():
+        finish(beyond)
 
     def late_back():
         finish(late)
@@ -552,19 +552,21 @@
     swapped(far)
     swapped(farther)
     straight(beside)
-    straight(beyond)
+    pl.when(inner == 1)(beyond_plane)
     finish(far)
     pl.when(inner == 1)(relay)
     finish(farther)
     for k in last + latest:
         pass_on(k)
     finish(beside)
-    finish(beyond)
+    pl.when(inner == 1)(beyond_back)
     swapped(last)
     swapped(latest)
+    pl.when(inner == 0)(beyond_plane)
+    finish(last)
     pl.when(inner == 1)(late_plane)
-    for k in last + latest:
-        finish_one(k)
+    finish(latest)
+    pl.when(inner == 0)(beyond_back)
     pl.when(inner == 1)(late_back)
     landed(returned.at[pl.ds(0, (n - 1) * capacity)], ret_recv.at[0])
     moe_out_ref[...] = jnp.dot(
@@ -605,7 +607,7 @@
     vmem = pl.BlockSpec(memory_space=pltpu.VMEM)
     hbm = pl.BlockSpec(memory_space=pl.ANY)
     dma = pltpu.SemaphoreType.DMA
-    return pl.pallas_call(
+    in_vmem = pl.pallas_call(
         functools.partial(
             fused_kernel, n, capacity, expert_count // group_router.shape[1]
         ),
@@ -639,9 +641,9 @@
             dma((5,)),
             dma((2,)),
             dma((6,)),
-            dma((n // 2 + n // 4,)),
+            dma((n // 2 + n // 4 + 1,)),
             dma((n // 4,)),
-            dma((n // 2 + n // 8,)),
+            dma((n,)),
             dma((1,)),
             dma((5,)),
         ],
@@ -663,6 +665,24 @@
         up_weight,
         down_weight,
     )
+    return pl.pallas_call(
+        write_out,
+        out_shape=tuple(jax.ShapeDtypeStruct(value.shape, value.dtype) for value in in_vmem),
+        in_specs=[hbm, hbm],
+        out_specs=(hbm, hbm),
+        scratch_shapes=[dma((2,))],
+    )(*[pltpu.with_memory_space_constraint(value, pltpu.VMEM) for value in in_vmem])
+
+
+def write_out(mix_vmem, moe_vmem, mix_hbm, moe_hbm, sem):
+    copies = [
+        pltpu.make_async_copy(mix_vmem, mix_hbm, sem.at[0]),
+        pltpu.make_async_copy(moe_vmem, moe_hbm, sem.at[1]),
+    ]
+    for copy in copies:
+        copy.start()
+    for copy in copies:
+        copy.wait()
 
 
 def step(*arrays):

time: 56.1 us -> 54.4 us (0.970)
  local copies, waits for them, and re-layouts: 1.67 us -> 0 us
    unnamed x2 -> x0, local copies, waits for them, and re-layouts: 1.67 us -> none
    pallas_call x1, Pallas kernels: 53.5 us -> 52 us  [fused(): pl.pallas_call(functools.partial(fused_kernel, n, capacity, expert_count...]
    pallas_call x0 -> x1, Pallas kernels: none -> 1.07 us  [fused(): pl.pallas_call(write_out, out_shape=tuple((jax.ShapeDtypeStruct(value.sha...]
where the time goes in v4:
time: 54.4 us; the launch traced here: 53.7 us
  Pallas kernels  53 us (97%)
  between operations  0.64 us (1%)
    pallas_call x1, Pallas kernels, fused(): pl.pallas_call(functools.partial(fused_kernel, n, capacity, expert_count...  52 us

profile of v4, /device:TPU:0, one launch (start us, length us, event | category | flops | bytes accessed | tf_op | source)
XLA Modules:
  0.0 53.7 jit_solution(6019518393036941653)
XLA Ops:
  0.6 52.0 %shard_map.140 = (bf16[256,2048]{1,0:T(8,128)(2,1)S(1)}, bf16[128,1024]{1,0:T(8,128)(2,1)S(1)}) custom-call(bf16[256,1024]{1,0:T(8,128)(2,1)} %mix_ref.1, bf16[8,128,128]{2,1,0:T(8,128)(2,1)} %pool_w_ref.1, f32[1,1024]{1,0:T(1,128)} %bitcast.9, bf16[1024,2048]{1,0:T(8,128)(2,1)} %out_w_hbm.1, bf16[128,2048]{1,0:T(8,128)(2,1)} %moe_ref.1, f32[1,2048]{1,0:T(1,128)} %bitcast.8, ...), custom_call_target="tpu_custom_call" | custom-call | tf_op jit(solution)/shard_map/pallas_call | solution.py:610
  52.6 1.1 %shard_map.141 = (bf16[256,2048]{1,0:T(8,128)(2,1)}, bf16[128,1024]{1,0:T(8,128)(2,1)}) custom-call(bf16[256,2048]{1,0:T(8,128)(2,1)S(1)} %get-tuple-element.4.mix_vmem, bf16[128,1024]{1,0:T(8,128)(2,1)S(1)} %get-tuple-element.5.moe_vmem), custom_call_target="tpu_custom_call" | custom-call | tf_op jit(solution)/shard_map/pallas_call | solution.py:668

commit v5 on v4

--- a/solution.py
+++ b/solution.py
@@ -169,21 +169,31 @@
     n,
     capacity,
     per_group,
-    mix_ref,
-    pool_w_ref,
-    pool_s_ref,
+    mix_hbm,
+    pool_w_hbm,
+    pool_s_hbm,
     out_w_hbm,
-    moe_ref,
-    gain_ref,
-    group_rt_ref,
-    inner_rt_ref,
-    gp_ref,
-    ip_ref,
+    moe_hbm,
+    gain_hbm,
+    group_rt_hbm,
+    inner_rt_hbm,
+    gp_hbm,
+    ip_hbm,
     gate_hbm,
     up_hbm,
     down_hbm,
     mix_out_ref,
     moe_out_ref,
+    moe_ref,
+    gain_ref,
+    gp_ref,
+    ip_ref,
+    mix_ref,
+    group_rt_ref,
+    inner_rt_ref,
+    pool_w_ref,
+    pool_s_ref,
+    input_sem,
     out_w,
     gate_w,
     up_w,
@@ -233,6 +243,24 @@
     for device in greeted:
         pl.semaphore_signal(barrier, inc=1, device_id=device, device_id_type=MESH)
 
+    inputs = [
+        pltpu.make_async_copy(source, target, input_sem.at[index])
+        for index, (source, target) in enumerate(
+            [
+                (moe_hbm, moe_ref),
+                (gain_hbm, gain_ref),
+                (gp_hbm, gp_ref),
+                (ip_hbm, ip_ref),
+                (mix_hbm, mix_ref),
+                (group_rt_hbm, group_rt_ref),
+                (inner_rt_hbm, inner_rt_ref),
+                (pool_w_hbm, pool_w_ref),
+                (pool_s_hbm, pool_s_ref),
+            ]
+        )
+    ]
+    for load in inputs:
+        load.start()
     loads = [
         pltpu.make_async_copy(gate_hbm.at[0], gate_w, load_sem.at[0]),
         pltpu.make_async_copy(up_hbm.at[0], up_w, load_sem.at[1]),
@@ -243,6 +271,8 @@
     for index in (0, 1, 3, 4, 2):
         loads[index].start()
 
+    for load in inputs[:4]:
+        load.wait()
     values = moe_ref[...].astype(jnp.float32)
     scale = lax.rsqrt(
         jnp.maximum(jnp.sum(values * values, axis=1, keepdims=True) * (1.0 / width), NORM_FLOOR)
@@ -287,9 +317,10 @@
         device_id=(following // 2, following % 2),
         device_id_type=MESH,
     )
+    inputs[4].wait()
     halo_copy.start()
 
-    relay_lanes = [slice(first, first + half // 2) for first in range(0, half, half // 2)]
+    relay_lanes = [slice(0, half)]
 
     def rows_of(index):
         return pl.ds(pl.multiple_of(index * capacity, capacity), capacity)
@@ -419,6 +450,8 @@
     def logits_of(router):
         return contract(router[:, :half], normed_v[0]) + contract(router[:, half:], normed_v[1])
 
+    for load in inputs[5:]:
+        load.wait()
     group_logits = logits_of(group_rt_ref)
     inner_logits = logits_of(inner_rt_ref)
     group_ids = lax.broadcasted_iota(jnp.int32, group_logits.shape, 0)
@@ -615,9 +648,19 @@
             pltpu.VMEM((rows, out_weight.shape[1]), bf16),
             pltpu.VMEM((tokens, half), bf16),
         ),
-        in_specs=[vmem, vmem, vmem, hbm] + [vmem] * 6 + [hbm] * 3,
+        in_specs=[hbm] * 13,
         out_specs=(vmem, vmem),
         scratch_shapes=[
+            pltpu.VMEM((tokens, width), bf16),
+            pltpu.VMEM((1, width), moe_gain.dtype),
+            pltpu.VMEM((1, tokens), group_pick.dtype),
+            pltpu.VMEM((inner_pick.shape[1], tokens), inner_pick.dtype),
+            pltpu.VMEM((rows, channels), bf16),
+            pltpu.VMEM(group_router.T.shape, bf16),
+            pltpu.VMEM(inner_router.T.shape, bf16),
+            pltpu.VMEM(pool_weight.shape, bf16),
+            pltpu.VMEM((1, channels), pool_scale.dtype),
+            dma((9,)),
             pltpu.VMEM(out_weight.shape, bf16),
             pltpu.VMEM((width, hidden), bf16),
             pltpu.VMEM((width, hidden), bf16),

time: 54.4 us -> 53.6 us (0.985)
  no operation moved by 1% of the time
where the time goes in v5:
time: 53.6 us; the launch traced here: 53.1 us
  Pallas kernels  52.5 us (98%)
  between operations  0.64 us (1%)
    pallas_call x1, Pallas kernels, fused(): pl.pallas_call(functools.partial(fused_kernel, n, capacity, expert_count...  51.4 us

profile of v5, /device:TPU:0, one launch (start us, length us, event | category | flops | bytes accessed | tf_op | source)
XLA Modules:
  0.0 53.1 jit_solution(10773994176250583297)
XLA Ops:
  0.6 51.4 %shard_map.140 = (bf16[256,2048]{1,0:T(8,128)(2,1)S(1)}, bf16[128,1024]{1,0:T(8,128)(2,1)S(1)}) custom-call(bf16[256,1024]{1,0:T(8,128)(2,1)} %mix_hbm.1, bf16[8,128,128]{2,1,0:T(8,128)(2,1)} %pool_w_hbm.1, f32[1,1024]{1,0:T(1,128)} %bitcast.9, bf16[1024,2048]{1,0:T(8,128)(2,1)} %out_w_hbm.1, bf16[128,2048]{1,0:T(8,128)(2,1)} %moe_hbm.1, f32[1,2048]{1,0:T(1,128)} %bitcast.8, ...), custom_call_target="tpu_custom_call" | custom-call | tf_op jit(solution)/shard_map/pallas_call | solution.py:643
  52.1 1.1 %shard_map.141 = (bf16[256,2048]{1,0:T(8,128)(2,1)}, bf16[128,1024]{1,0:T(8,128)(2,1)}) custom-call(bf16[256,2048]{1,0:T(8,128)(2,1)S(1)} %get-tuple-element.4.mix_vmem, bf16[128,1024]{1,0:T(8,128)(2,1)S(1)} %get-tuple-element.5.moe_vmem), custom_call_target="tpu_custom_call" | custom-call | tf_op jit(solution)/shard_map/pallas_call | solution.py:711
